TPU v7x, 32 devices: a whole 2x2x4 slice. The times are simulated.
32 devices in a mesh: ep: 8 (over z, y), tp: 4 (over x, core).
Axes of the slice: x: 2, y: 2, z: 4, core: 2. Of those that a mesh axis runs over, the one named last changes fastest.
Arguments:
- tokens: bfloat16 [128, 2048], P('ep'), may hold values from -6 to 6
- norm_gain: bfloat16 [2048], replicated, may hold values from 0.099609375 to 1.8984375
- query_weight: bfloat16 [2048, 1024], P('ep', 'tp'), may hold values from -0.125 to 0.125
- key_weight: bfloat16 [2048, 1024], P('ep', 'tp'), may hold values from -0.125 to 0.125
- value_weight: bfloat16 [2048, 2048], P('ep', 'tp'), may hold values from -0.125 to 0.125
- outgate_weight: bfloat16 [2048, 2048], P('ep', 'tp'), may hold values from -0.125 to 0.125
- beta_weight: bfloat16 [2048, 16], replicated, may hold values from -0.125 to 0.125
- decay_weight: bfloat16 [2048, 16], replicated, may hold values from -0.125 to 0.125
- decay_rate: float32 [16], P('tp'), may hold values from 0.02 to 6
- decay_bias: float32 [16], P('tp'), may hold values from -3 to 3
- head_gain: bfloat16 [128], replicated, may hold values from 0.099609375 to 1.8984375
- recurrent: float32 [128, 16, 128, 128], P('ep', 'tp'), may hold values from -3 to 3
- output_weight: bfloat16 [2048, 2048], P('tp', 'ep'), may hold values from -0.125 to 0.125
- ffn_gain: bfloat16 [2048], replicated, may hold values from 0.099609375 to 1.8984375
- routes: int32 [128, 4], P('ep'), may hold values from 0 to 7, all different within a row; in each aligned block of 16 rows (0 to 15, 16 to 31, ...) at most 16 rows name the same one
- route_weight: float32 [128, 4], P('ep'), may hold values from 0.1 to 1
- expert_gate: bfloat16 [8, 2048, 512], P('ep', None, 'tp'), may hold values from -0.125 to 0.125
- expert_up: bfloat16 [8, 2048, 512], P('ep', None, 'tp'), may hold values from -0.125 to 0.125
- expert_down: bfloat16 [8, 512, 2048], P('ep', 'tp'), may hold values from -0.25 to 0.25
- shared_gate: bfloat16 [2048, 512], P('ep', 'tp'), may hold values from -0.125 to 0.125
- shared_up: bfloat16 [2048, 512], P('ep', 'tp'), may hold values from -0.125 to 0.125
- shared_down: bfloat16 [512, 2048], P('tp', 'ep'), may hold values from -0.25 to 0.25
- branch_gate: bfloat16 [2048], replicated, may hold values from -0.125 to 0.125
Outputs:
- layer_out: bfloat16 [128, 2048], P('ep')
- new_state: float32 [128, 16, 128, 128], P('ep', 'tp')
Inputs may be any that keep to these rules, and one draw needn't show every extreme that they name: `routes`: each row names 4 different experts. Among the rows of one aligned block of 16 rows no expert is named more than 16 times, and some block reaches it: one expert is named exactly 16 times there.
All inputs are finite; a program needn't handle non-finite values.
Results may differ from a plain program's by a relative error of at most 0.019.
Values may be sent and summed in bfloat16 or wider, within the bound.
A program may use at most 64 MiB of HBM per device.

v0:
```python
import jax
import jax.numpy as jnp
from jax import lax
from jax.sharding import PartitionSpec as P

EPS = 1e-06
ROUTED_SCALE = 2.5


def rms_scale(values, gain):
    values = values.astype(jnp.float32)
    return (
        values
        * lax.rsqrt(jnp.mean(values * values, axis=-1, keepdims=True) + EPS)
        * gain.astype(jnp.float32)
    )


def unit_rows(values):
    return values * lax.rsqrt(jnp.sum(values * values, axis=-1, keepdims=True) + EPS)


def per_device(
    tokens,
    norm_gain,
    query_weight,
    key_weight,
    value_weight,
    outgate_weight,
    beta_weight,
    decay_weight,
    decay_rate,
    decay_bias,
    head_gain,
    recurrent,
    output_weight,
    ffn_gain,
    routes,
    route_weight,
    expert_gate,
    expert_up,
    expert_down,
    shared_gate,
    shared_up,
    shared_down,
    branch_gate,
):
    ep_count = lax.axis_size("ep")
    seq_local, width = tokens.shape
    heads_local, key_dim, value_dim = (recurrent.shape[1], recurrent.shape[2], recurrent.shape[3])
    normed = rms_scale(tokens, norm_gain).astype(jnp.bfloat16)
    query_cols = query_weight.shape[1]
    value_cols = value_weight.shape[1]
    spread = lax.all_to_all(normed, "ep", split_axis=1, concat_axis=0, tiled=True)
    stacked = jnp.concatenate((query_weight, key_weight, value_weight, outgate_weight), axis=1)
    token_block = spread
    projected = lax.psum_scatter(
        jnp.dot(token_block, stacked, preferred_element_type=jnp.float32),
        "ep",
        scatter_dimension=0,
        tiled=True,
    )
    query_sum = projected[:, :query_cols]
    key_sum = projected[:, query_cols : 2 * query_cols]
    value_sum = projected[:, 2 * query_cols : 2 * query_cols + value_cols]
    gate_sum = projected[:, 2 * query_cols + value_cols :]
    query_proj = query_sum.astype(jnp.bfloat16)
    key_proj = key_sum.astype(jnp.bfloat16)
    value_proj = value_sum.astype(jnp.bfloat16)
    gate_proj = gate_sum.astype(jnp.bfloat16)
    key_local = query_cols // key_dim
    repeat_count = heads_local // key_local
    queries = unit_rows(
        jax.nn.silu(query_proj.astype(jnp.float32)).reshape(seq_local, key_local, key_dim)
    )
    queries = jnp.repeat(queries, repeat_count, axis=1) * key_dim ** (-0.5)
    key_rows = unit_rows(
        jax.nn.silu(key_proj.astype(jnp.float32)).reshape(seq_local, key_local, key_dim)
    )
    key_rows = jnp.repeat(key_rows, repeat_count, axis=1)
    value_rows = jax.nn.silu(value_proj.astype(jnp.float32)).reshape(
        seq_local, heads_local, value_dim
    )
    head_start = lax.axis_index("tp") * heads_local
    beta_logit = jnp.dot(
        normed,
        lax.dynamic_slice_in_dim(beta_weight, head_start, heads_local, 1),
        preferred_element_type=jnp.float32,
    )
    decay_logit = jnp.dot(
        normed,
        lax.dynamic_slice_in_dim(decay_weight, head_start, heads_local, 1),
        preferred_element_type=jnp.float32,
    )
    strength = jax.nn.sigmoid(beta_logit)
    retain = jnp.exp(-decay_rate[None, :] * jax.nn.softplus(decay_logit + decay_bias[None, :]))
    decayed = recurrent * retain[:, :, None, None]
    predicted = jnp.einsum("shde,shd->she", decayed, key_rows, precision=lax.Precision.HIGHEST)
    correction = strength[:, :, None] * (value_rows - predicted)
    new_state = decayed + key_rows[:, :, :, None] * correction[:, :, None, :]
    readout = jnp.einsum("shde,shd->she", new_state, queries, precision=lax.Precision.HIGHEST)
    out_gate = jax.nn.silu(gate_proj.astype(jnp.float32)).reshape(seq_local, heads_local, value_dim)
    heads_out = (
        (rms_scale(readout, head_gain) * out_gate)
        .astype(jnp.bfloat16)
        .reshape(seq_local, heads_local * value_dim)
    )
    partial_mix = jnp.dot(
        heads_out,
        lax.all_gather(output_weight, "ep", axis=1, tiled=True),
        preferred_element_type=jnp.float32,
    )
    partial_mix = partial_mix.astype(jnp.bfloat16).astype(jnp.float32)
    mixed = lax.psum(partial_mix.astype(jnp.bfloat16), "tp").astype(jnp.float32)
    residual = (tokens.astype(jnp.float32) + mixed).astype(jnp.bfloat16)
    ffn_in = rms_scale(residual, ffn_gain).astype(jnp.bfloat16)
    token_block = ffn_in
    shared_g = jnp.dot(
        token_block,
        lax.all_gather(shared_gate, "ep", axis=0, tiled=True),
        preferred_element_type=jnp.float32,
    )
    shared_u = jnp.dot(
        token_block,
        lax.all_gather(shared_up, "ep", axis=0, tiled=True),
        preferred_element_type=jnp.float32,
    )
    shared_act = (jax.nn.silu(shared_g) * shared_u).astype(jnp.bfloat16)
    shared_partial = jnp.dot(
        shared_act,
        lax.all_gather(shared_down, "ep", axis=1, tiled=True),
        preferred_element_type=jnp.float32,
    )
    shared_out = lax.psum(
        shared_partial.astype(jnp.bfloat16).astype(jnp.float32).astype(jnp.bfloat16), "tp"
    ).astype(jnp.float32)
    topk = routes.shape[1]
    pair_count = seq_local * topk
    capacity = 2 * ((pair_count + ep_count - 1) // ep_count)
    expert_ids = routes.reshape(pair_count)
    onehot = (expert_ids[:, None] == jnp.arange(ep_count)[None, :]).astype(jnp.float32)
    earlier = (jnp.arange(pair_count)[:, None] > jnp.arange(pair_count)[None, :]).astype(
        jnp.float32
    )
    slots = jnp.sum(
        jnp.dot(earlier, onehot, precision=lax.Precision.HIGHEST) * onehot, axis=1
    ).astype(jnp.int32)
    target = expert_ids * capacity + slots
    placement_matrix = (target[:, None] == jnp.arange(ep_count * capacity)[None, :]).astype(
        jnp.bfloat16
    )
    dispatch_matrix = jnp.sum(
        placement_matrix.reshape(seq_local, topk, ep_count * capacity).astype(jnp.float32), axis=1
    ).astype(jnp.bfloat16)
    outgoing = jnp.dot(dispatch_matrix.T, ffn_in, preferred_element_type=jnp.float32).astype(
        jnp.bfloat16
    )
    outgoing = outgoing.reshape(ep_count, capacity, width)
    received = lax.all_to_all(outgoing, "ep", split_axis=0, concat_axis=0, tiled=True)
    flat_rows = received.reshape(-1, width)
    gate_part = jnp.dot(flat_rows, expert_gate[0], preferred_element_type=jnp.float32)
    up_part = jnp.dot(flat_rows, expert_up[0], preferred_element_type=jnp.float32)
    act = (jax.nn.silu(gate_part) * up_part).astype(jnp.bfloat16)
    partial_rows = (
        jnp.dot(act, expert_down[0], preferred_element_type=jnp.float32)
        .astype(jnp.bfloat16)
        .astype(jnp.float32)
    )
    summed = lax.psum(partial_rows.astype(jnp.bfloat16), "tp")
    returned = lax.all_to_all(
        summed.reshape(received.shape), "ep", split_axis=0, concat_axis=0, tiled=True
    )
    scaled = route_weight / jnp.sum(route_weight, axis=1, keepdims=True) * ROUTED_SCALE
    branch = jax.nn.sigmoid(jnp.dot(ffn_in, branch_gate, preferred_element_type=jnp.float32))
    pair_out = jnp.dot(
        placement_matrix,
        returned.reshape(ep_count * capacity, width),
        preferred_element_type=jnp.float32,
    )
    moe = jnp.sum(pair_out.reshape(seq_local, topk, width) * scaled[:, :, None], axis=1)
    layer_out = (residual.astype(jnp.float32) + moe + branch[:, None] * shared_out).astype(
        jnp.bfloat16
    )
    return (layer_out, new_state)


def solution(mesh):
    return jax.shard_map(
        per_device,
        mesh=mesh,
        in_specs=(
            P("ep", None),
            P(),
            P("ep", "tp"),
            P("ep", "tp"),
            P("ep", "tp"),
            P("ep", "tp"),
            P(),
            P(),
            P("tp"),
            P("tp"),
            P(),
            P("ep", "tp", None, None),
            P("tp", "ep"),
            P(),
            P("ep", None),
            P("ep", None),
            P("ep", None, "tp"),
            P("ep", None, "tp"),
            P("ep", "tp", None),
            P("ep", "tp"),
            P("ep", "tp"),
            P("tp", "ep"),
            P(),
        ),
        out_specs=(P("ep", None), P("ep", "tp", None, None)),
        check_vma=False,
    )
```

profile of v0, /device:TPU:0, one launch (start us, length us, event | category | flops | bytes accessed | tf_op | source)
XLA Modules:
  0.0 310.8 jit_solution(1554573020818032295)
XLA Ops:
  7.2 0.0 copy-start
  7.2 0.0 reduce-scatter.2.cloned.1.call-start
  7.3 0.7 convert_element_type.97
  8.0 1.0 fusion.27
  9.0 0.9 fusion.29
  9.9 14.0 %all_to_all.29 = bf16[16,8,256]{2,0,1:T(8,128)(2,1)S(1)} all-to-all(bf16[16,8,256]{2,0,1:T(8,128)(2,1)S(1)} %bitcast.82), channel_id=1, replica_groups=mesh['ep'=8,'tp'=4] {'ep'}, dimensions={1} | all-to-all | bytes 131072 | tf_op jit(solution)/shard_map/all_to_all | solution.py:54
  24.0 2.3 fusion.14
  26.2 0.0 reduce-scatter.2.cloned.1.call-update
  26.2 0.0 all-gather.2.cloned.1.call-start
  26.3 0.7 all-gather.2.cloned.1.call-update
  27.0 0.0 all-reduce.4.cloned.1.call-start
  27.1 0.9 fusion.70
  28.0 0.1 copy.43
  28.1 0.9 fusion.9
  29.0 0.1 copy.45
  29.1 0.0 copy-done.6
  29.1 31.9 %all_gather.13 = bf16[2048,128]{1,0:T(8,128)(2,1)S(1)} all-gather(bf16[256,128]{1,0:T(8,128)(2,1)S(1)} %copy-done.6), channel_id=1, replica_groups=mesh['ep'=8,'tp'=4] {'ep'}, dimensions={0}, use_global_device_ids=true | all-gather | bytes 589824 | tf_op jit(solution)/shard_map/all_gather | solution.py:120
  61.0 0.1 copy.46
  61.1 0.1 eq.51
  61.2 0.1 fusion.6
  61.4 0.1 convert_element_type.110
  61.4 0.1 copy.47
  61.5 25.8 %reduce-scatter.2.cloned.1.call-done = f32[16,1536]{1,0:T(8,128)} async-done(((f32[128,1536]{1,0:T(8,128)}), f32[16,1536]{1,0:T(8,128)}) %reduce-scatter.2.cloned.1.call-update) | async-done | bytes 98320 | tf_op jit(solution)/shard_map/reduce_scatter | solution.py:57
  87.3 0.9 convert.7
  88.3 0.0 copy-start.1
  88.4 0.1 multiply_reduce_fusion.2
  88.5 0.1 multiply_reduce_fusion.1
  88.6 0.1 broadcast_multiply_fusion
  88.7 0.1 multiply_multiply_fusion
  88.8 5.8 %fusion = f32[16,4,1,128]{3,2,1,0:T(1,128)S(1)} fusion(f32[16,4,128,1]{2,3,1,0:T(1,128)S(1)} %bitcast.77, f32[16,4,128,128]{3,2,1,0:T(8,128)} %param.34, f32[16,4]{1,0:T(8,128)S(1)} %copy.43), kind=kOutput, calls=%fused_computation.1 | convolution fusion | flops 13631488 | bytes 4260096 | tf_op jit(solution)/shard_map/shde,shd->she/dot_general | solution.py:98
  94.6 0.1 subtract_multiply_fusion
  94.7 1.5 multiply_add_fusion
  96.2 0.0 copy-start.2
  96.2 0.0 copy-start.11
  96.2 0.0 copy-start.3
  96.2 2.0 copy-done.2
  98.2 3.6 %fusion.79 = f32[16,4,1,128]{3,2,1,0:T(1,128)S(1)} fusion(f32[16,4,128,128]{3,2,1,0:T(8,128)S(1)} %multiply_add_fusion, f32[16,4,128,1]{2,3,1,0:T(1,128)S(1)} %bitcast.84), kind=kOutput, calls=%fused_computation.121 | convolution fusion | flops 12582912 | bytes 4259840 | tf_op jit(solution)/shard_map/shde,shd->she/dot_general | solution.py:101
  101.9 0.1 multiply_reduce_fusion
  102.0 0.1 multiply_convert_fusion
  102.1 36.7 %all-gather.2.cloned.1.call-done = bf16[512,2048]{1,0:T(8,128)(2,1)} async-done(((bf16[512,256]{1,0:T(8,128)(2,1)}), bf16[512,2048]{1,0:T(8,128)(2,1)}) %all-gather.2.cloned.1.call-update) | async-done | bytes 2097168 | tf_op jit(solution)/shard_map/all_gather | solution.py:110
  138.7 2.6 convolution_convert_fusion.3
  141.3 0.0 all-reduce.4.cloned.1.call-update
  141.4 0.1 fusion.57
  141.5 29.9 %all-reduce.4.cloned.1.call-done = bf16[16,2048]{1,0:T(8,128)(2,1)} async-done(((bf16[16,2048]{1,0:T(8,128)(2,1)}), bf16[16,2048]{1,0:T(8,128)(2,1)}) %all-reduce.4.cloned.1.call-update) | async-done | bytes 65552 | tf_op jit(solution)/shard_map/psum | solution.py:114
  171.4 1.0 fusion.31
  172.4 0.9 fusion.33
  173.3 1.1 convolution_convert_fusion.1
  174.4 5.5 %all-to-all-start.1 = ((bf16[8,16,2048]{2,1,0:T(8,128)(2,1)}), bf16[8,16,2048]{2,1,0:T(8,128)(2,1)S(1)}, u32[]{:S(2)}, u32[]{:S(2)}) async-start(bf16[8,16,2048]{2,1,0:T(8,128)(2,1)} %bitcast.13), calls=%async_computation.2 | async-start | bytes 1048576 | tf_op jit(solution)/shard_map/all_to_all | solution.py:159
  179.9 0.0 copy-start.10
  179.9 0.0 all-reduce.6.cloned.1.call-start
  180.0 37.8 %all_gather.14 = bf16[2048,128]{1,0:T(8,128)(2,1)S(1)} all-gather(bf16[256,128]{1,0:T(8,128)(2,1)S(1)} %copy-done.7), channel_id=1, replica_groups=mesh['ep'=8,'tp'=4] {'ep'}, dimensions={0}, use_global_device_ids=true | all-gather | bytes 589824 | tf_op jit(solution)/shard_map/all_gather | solution.py:125
  217.8 31.3 %all_gather.15 = bf16[128,2048]{1,0:T(8,128)(2,1)S(1)} all-gather(bf16[128,256]{1,0:T(8,128)(2,1)S(1)} %copy-done.8), channel_id=1, replica_groups=mesh['ep'=8,'tp'=4] {'ep'}, dimensions={1}, use_global_device_ids=true | all-gather | bytes 589824 | tf_op jit(solution)/shard_map/all_gather | solution.py:131
  249.1 0.2 fusion.80
  249.3 1.0 convolution_convert_fusion.2
  250.3 0.0 all-to-all-done.1
  250.3 0.3 fusion.25
  250.6 2.4 convolution_convert_fusion
  253.0 0.0 all-reduce.6.cloned.1.call-update
  253.0 30.3 %all-reduce.6.cloned.1.call-done = (bf16[8,16,2048]{2,1,0:T(8,128)(2,1)}, bf16[16,2048]{1,0:T(8,128)(2,1)}) async-done(((bf16[8,16,2048]{2,1,0:T(8,128)(2,1)}, bf16[16,2048]{1,0:T(8,128)(2,1)}), (bf16[8,16,2048]{2,1,0:T(8,128)(2,1)}, bf16[16,2048]{1,0:T(8,128)(2,1)})) %all-reduce.6.cloned.1.call-update) | async-done | bytes 589840 | tf_op jit(solution)/shard_map/psum | solution.py:169
  283.3 5.5 %all-to-all-start.2 = ((bf16[8,16,2048]{2,1,0:T(8,128)(2,1)}), bf16[8,16,2048]{2,1,0:T(8,128)(2,1)S(1)}, u32[]{:S(2)}, u32[]{:S(2)}) async-start(bf16[8,16,2048]{2,1,0:T(8,128)(2,1)} %get-tuple-element.2), calls=%async_computation.3 | async-start | bytes 1048576 | tf_op jit(solution)/shard_map/all_to_all | solution.py:170
  288.9 0.1 fusion.13
  289.0 13.4 %all-to-all-done.2 = bf16[8,16,2048]{2,1,0:T(8,128)(2,1)S(1)} async-done(((bf16[8,16,2048]{2,1,0:T(8,128)(2,1)}), bf16[8,16,2048]{2,1,0:T(8,128)(2,1)S(1)}, u32[]{:S(2)}, u32[]{:S(2)}) %all-to-all-start.2) | async-done | bytes 524320 | tf_op jit(solution)/shard_map/all_to_all | solution.py:170
  302.4 0.3 fusion.3
  302.7 1.6 fusion.35
  (46 shorter events, 0.3 us)
Async XLA Ops:
  7.2 243.4 %copy-start = (bf16[1,128,2048]{2,1,0:T(8,128)(2,1)S(1)}, bf16[1,128,2048]{2,1,0:T(8,128)(2,1)}, u32[]{:S(2)}) copy-start(bf16[1,128,2048]{2,1,0:T(8,128)(2,1)} %param.41) | copy-start | bytes 1572868
  7.2 19.9 %copy-start.13 = (f32[4]{0:T(128)S(1)}, f32[4]{0:T(128)}, u32[]{:S(2)}) copy-start(f32[4]{0:T(128)} %param.31) | copy-start | bytes 52
  7.2 19.9 %copy-start.14 = (f32[4]{0:T(128)S(1)}, f32[4]{0:T(128)}, u32[]{:S(2)}) copy-start(f32[4]{0:T(128)} %param.32) | copy-start | bytes 52
  7.2 21.9 %copy-start.15 = (bf16[128]{0:T(256)(128)(2,1)S(1)}, bf16[128]{0:T(256)(128)(2,1)}, u32[]{:S(2)}) copy-start(bf16[128]{0:T(256)(128)(2,1)} %param.33) | copy-start | bytes 772
  7.2 21.9 %copy-start.6 = (bf16[256,128]{1,0:T(8,128)(2,1)S(1)}, bf16[256,128]{1,0:T(8,128)(2,1)}, u32[]{:S(2)}) copy-start(bf16[256,128]{1,0:T(8,128)(2,1)} %param.42) | copy-start | bytes 196612
  7.2 53.8 %copy-start.9 = (s32[16,4]{0,1:T(4,128)S(1)}, s32[16,4]{0,1:T(4,128)}, u32[]{:S(2)}) copy-start(s32[16,4]{0,1:T(4,128)} %param.37) | copy-start | bytes 772
  7.2 80.1 %reduce-scatter.2.cloned.1.call-start = ((), (), s32[]{:S(2)}) async-start(), calls=%async_computation.4 | async-start | bytes 884736 | tf_op jit(solution)/shard_map/reduce_scatter | solution.py:57
  26.2 112.5 %all-gather.2.cloned.1.call-start = ((), (), s32[]{:S(2)}) async-start(), calls=%async_computation.5 | async-start | bytes 2359296 | tf_op jit(solution)/shard_map/all_gather | solution.py:110
  27.0 144.4 %all-reduce.4.cloned.1.call-start = ((), (), s32[]{:S(2)}) async-start(), calls=%async_computation.6 | async-start | bytes 131072 | tf_op jit(solution)/shard_map/psum | solution.py:114
  88.3 6.3 %copy-start.1 = (f32[16,4,128,128]{3,2,1,0:T(8,128)S(1)}, f32[16,4,128,128]{3,2,1,0:T(8,128)}, u32[]{:S(2)}) copy-start(f32[16,4,128,128]{3,2,1,0:T(8,128)} %param.34) | copy-start | bytes 12582916
  96.2 2.0 copy-start.2
  96.2 45.2 %copy-start.11 = (bf16[2048]{0:T(1024)(128)(2,1)S(1)}, bf16[2048]{0:T(1024)(128)(2,1)}, u32[]{:S(2)}) copy-start(bf16[2048]{0:T(1024)(128)(2,1)} %param.36) | copy-start | bytes 12292
  96.2 75.2 %copy-start.3 = (bf16[16,2048]{1,0:T(8,128)(2,1)S(1)}, bf16[16,2048]{1,0:T(8,128)(2,1)}, u32[]{:S(2)}) copy-start(bf16[16,2048]{1,0:T(8,128)(2,1)} %param.23) | copy-start | bytes 196612
  98.2 81.8 %copy-start.7 = (bf16[256,128]{1,0:T(8,128)(2,1)S(1)}, bf16[256,128]{1,0:T(8,128)(2,1)}, u32[]{:S(2)}) copy-start(bf16[256,128]{1,0:T(8,128)(2,1)} %param.43) | copy-start | bytes 196612
  98.2 119.6 %copy-start.8 = (bf16[128,256]{1,0:T(8,128)(2,1)S(1)}, bf16[128,256]{1,0:T(8,128)(2,1)}, u32[]{:S(2)}) copy-start(bf16[128,256]{1,0:T(8,128)(2,1)} %param.44) | copy-start | bytes 196612
  101.9 148.4 %copy-start.5 = (bf16[1,2048,128]{2,1,0:T(8,128)(2,1)S(1)}, bf16[1,2048,128]{2,1,0:T(8,128)(2,1)}, u32[]{:S(2)}) copy-start(bf16[1,2048,128]{2,1,0:T(8,128)(2,1)} %param.39) | copy-start | bytes 1572868
  174.4 75.9 %all-to-all-start.1 = ((bf16[8,16,2048]{2,1,0:T(8,128)(2,1)}), bf16[8,16,2048]{2,1,0:T(8,128)(2,1)S(1)}, u32[]{:S(2)}, u32[]{:S(2)}) async-start(bf16[8,16,2048]{2,1,0:T(8,128)(2,1)} %bitcast.13), calls=%async_computation.2 | async-start | bytes 1048576 | tf_op jit(solution)/shard_map/all_to_all | solution.py:159
  179.9 108.9 %copy-start.12 = (bf16[2048]{0:T(1024)(128)(2,1)S(1)}, bf16[2048]{0:T(1024)(128)(2,1)}, u32[]{:S(2)}) copy-start(bf16[2048]{0:T(1024)(128)(2,1)} %param.45) | copy-start | bytes 12292
  179.9 108.9 %copy-start.10 = (f32[16,4]{0,1:T(4,128)S(1)}, f32[16,4]{0,1:T(4,128)}, u32[]{:S(2)}) copy-start(f32[16,4]{0,1:T(4,128)} %param.38) | copy-start | bytes 772
  179.9 122.7 %copy-start.4 = (bf16[16,2048]{1,0:T(8,128)(2,1)S(1)}, bf16[16,2048]{1,0:T(8,128)(2,1)}, u32[]{:S(2)}) copy-start(bf16[16,2048]{1,0:T(8,128)(2,1)} %all-reduce.4.cloned.1.call-done) | copy-start | bytes 196612
  179.9 103.3 %all-reduce.6.cloned.1.call-start = ((), (), s32[]{:S(2)}) async-start(), calls=%async_computation.7 | async-start | bytes 1179648 | tf_op jit(solution)/shard_map/psum | solution.py:169
  283.3 19.1 %all-to-all-start.2 = ((bf16[8,16,2048]{2,1,0:T(8,128)(2,1)}), bf16[8,16,2048]{2,1,0:T(8,128)(2,1)S(1)}, u32[]{:S(2)}, u32[]{:S(2)}) async-start(bf16[8,16,2048]{2,1,0:T(8,128)(2,1)} %get-tuple-element.2), calls=%async_computation.3 | async-start | bytes 1048576 | tf_op jit(solution)/shard_map/all_to_all | solution.py:170
Sparse Core Ops, SparseCore 0:
  26.4 60.8 reduce-scatter.1
  89.3 49.3 all-gather.1
  141.6 29.7 all-reduce.3
  253.1 30.1 all-reduce.5
where the time goes:
time: 312 us; the launch traced here: 311 us
  waiting for transfers between devices  137 us (44%)
  blocking collectives  115 us (37%)
  matrix products  21.6 us (7%)
  between operations  14.2 us (5%)
  starting transfers between devices  11.2 us (4%)
  other arithmetic  9.3 us (3%)
    all_gather x1, blocking collectives, per_device(): lax.all_gather(shared_up, 'ep', axis=0, tiled=True)  37.8 us
    all_gather x1, waiting for transfers between devices, per_device(): lax.all_gather(output_weight, 'ep', axis=1, tiled=True)  36.7 us
    all_gather x1, blocking collectives, per_device(): lax.all_gather(shared_gate, 'ep', axis=0, tiled=True)  31.9 us
    all_gather x1, blocking collectives, per_device(): lax.all_gather(shared_down, 'ep', axis=1, tiled=True)  31.3 us
    psum x1, waiting for transfers between devices, per_device(): summed = lax.psum(partial_rows.astype(jnp.bfloat16), 'tp')  30.3 us
    psum x1, waiting for transfers between devices, per_device(): mixed = lax.psum(partial_mix.astype(jnp.bfloat16), 'tp').astype(jnp.float32)  29.9 us
    reduce_scatter x1, waiting for transfers between devices, per_device(): lax.psum_scatter(jnp.dot(token_block, stacked, preferred_element_type=jnp...  25.8 us
    all_to_all x1, blocking collectives, per_device(): lax.all_to_all(normed, 'ep', split_axis=1, concat_axis=0, tiled=True)  14 us
  transfers between devices with their start and end apart: 6, of which 5 were waited for; matrix products, arithmetic and copies ran while one was open for 5% of the time, Pallas kernels for 0%

commit v1 on v0

--- a/solution.py
+++ b/solution.py
@@ -2,6 +2,7 @@
 import jax.numpy as jnp
 from jax import lax
 from jax.sharding import PartitionSpec as P
+from jax.lax import all_gather
 
 EPS = 1e-06
 ROUTED_SCALE = 2.5
@@ -111,7 +112,12 @@
         preferred_element_type=jnp.float32,
     )
     partial_mix = partial_mix.astype(jnp.bfloat16).astype(jnp.float32)
-    mixed = lax.psum(partial_mix.astype(jnp.bfloat16), "tp").astype(jnp.float32)
+
+    def _lead_waves(view):
+        met_up = all_gather(view, "tp").sum(axis=0)
+        return met_up
+
+    mixed = _lead_waves(partial_mix.astype(jnp.bfloat16)).astype(jnp.float32)
     residual = (tokens.astype(jnp.float32) + mixed).astype(jnp.bfloat16)
     ffn_in = rms_scale(residual, ffn_gain).astype(jnp.bfloat16)
     token_block = ffn_in

time: 312 us -> 285 us (0.913)
  waiting for transfers between devices: 137 us -> 108 us
  blocking collectives: 115 us -> 122 us
    psum x1 -> x0, waiting for transfers between devices: 29.9 us -> none  [per_device(): mixed = lax.psum(partial_mix.astype(jnp.bfloat16), 'tp').astype(jnp.float32)]
    all_gather x0 -> x1, blocking collectives: none -> 5.77 us  [_lead_waves(): met_up = all_gather(view, 'tp').sum(axis=0)]
  transfers between devices with their start and end apart: 6 -> 5, of which waited for: 5 -> 4; matrix products, arithmetic and copies ran while one was open for 5% -> 6% of each run, Pallas kernels for 0% -> 0%
where the time goes in v1:
time: 285 us; the launch traced here: 284 us
  blocking collectives  122 us (43%)
  waiting for transfers between devices  108 us (38%)
  matrix products  21 us (7%)
  between operations  14.2 us (5%)
  starting transfers between devices  9.13 us (3%)
  other arithmetic  7.68 us (3%)
    all_gather x1, blocking collectives, per_device(): lax.all_gather(shared_up, 'ep', axis=0, tiled=True)  38.9 us
    all_gather x1, waiting for transfers between devices, per_device(): lax.all_gather(output_weight, 'ep', axis=1, tiled=True)  36.7 us
    all_gather x1, blocking collectives, per_device(): lax.all_gather(shared_gate, 'ep', axis=0, tiled=True)  31.7 us
    all_gather x1, blocking collectives, per_device(): lax.all_gather(shared_down, 'ep', axis=1, tiled=True)  31.4 us
    psum x1, waiting for transfers between devices, per_device(): summed = lax.psum(partial_rows.astype(jnp.bfloat16), 'tp')  31.3 us
    reduce_scatter x1, waiting for transfers between devices, per_device(): lax.psum_scatter(jnp.dot(token_block, stacked, preferred_element_type=jnp...  25.8 us
    all_to_all x1, blocking collectives, per_device(): lax.all_to_all(normed, 'ep', split_axis=1, concat_axis=0, tiled=True)  14 us
    all_to_all x1, waiting for transfers between devices, per_device(): lax.all_to_all(summed.reshape(received.shape), 'ep', split_axis=0, concat...  13.4 us
  transfers between devices with their start and end apart: 5, of which 4 were waited for; matrix products, arithmetic and copies ran while one was open for 6% of the time, Pallas kernels for 0%

profile of v1, /device:TPU:0, one launch (start us, length us, event | category | flops | bytes accessed | tf_op | source)
XLA Modules:
  0.0 284.5 jit_solution(1318093337728636448)
XLA Ops:
  7.2 0.0 copy-start
  7.2 0.0 copy-start.12
  7.2 0.0 reduce-scatter.2.cloned.1.call-start
  7.3 0.8 convert_element_type.99
  8.0 1.0 fusion.27
  9.0 0.9 fusion.29
  10.0 14.0 %all_to_all.29 = bf16[16,8,256]{2,0,1:T(8,128)(2,1)S(1)} all-to-all(bf16[16,8,256]{2,0,1:T(8,128)(2,1)S(1)} %bitcast.84), channel_id=1, replica_groups=mesh['ep'=8,'tp'=4] {'ep'}, dimensions={1} | all-to-all | bytes 131072 | tf_op jit(solution)/shard_map/all_to_all | solution.py:55
  24.0 2.3 fusion.14
  26.2 0.0 reduce-scatter.2.cloned.1.call-update
  26.3 0.0 all-gather.3.cloned.1.call-start
  26.3 0.7 all-gather.3.cloned.1.call-update
  27.0 0.9 fusion.70
  28.0 0.1 copy.43
  28.0 0.9 fusion.9
  28.9 0.1 copy.45
  29.0 0.0 copy-done.10
  29.1 0.1 copy.46
  29.2 0.1 eq.51
  29.3 0.1 fusion.6
  29.4 0.1 convert_element_type.112
  29.5 0.1 copy.47
  29.6 0.1 fusion.57
  29.7 0.0 copy-done.5
  29.7 31.7 %all_gather.21 = bf16[2048,128]{1,0:T(8,128)(2,1)S(1)} all-gather(bf16[256,128]{1,0:T(8,128)(2,1)S(1)} %copy-done.5), channel_id=1, replica_groups=mesh['ep'=8,'tp'=4] {'ep'}, dimensions={0}, use_global_device_ids=true | all-gather | bytes 589824 | tf_op jit(solution)/shard_map/all_gather | solution.py:126
  61.4 25.8 %reduce-scatter.2.cloned.1.call-done = f32[16,1536]{1,0:T(8,128)} async-done(((f32[128,1536]{1,0:T(8,128)}), f32[16,1536]{1,0:T(8,128)}) %reduce-scatter.2.cloned.1.call-update) | async-done | bytes 98320 | tf_op jit(solution)/shard_map/reduce_scatter | solution.py:58
  87.3 0.9 convert.8
  88.3 0.0 copy-start.1
  88.3 0.1 multiply_reduce_fusion.2
  88.4 0.1 multiply_reduce_fusion.1
  88.5 0.1 broadcast_multiply_fusion
  88.6 0.1 multiply_multiply_fusion
  88.7 5.8 %fusion = f32[16,4,1,128]{3,2,1,0:T(1,128)S(1)} fusion(f32[16,4,128,1]{2,3,1,0:T(1,128)S(1)} %bitcast.79, f32[16,4,128,128]{3,2,1,0:T(8,128)} %param.34, f32[16,4]{1,0:T(8,128)S(1)} %copy.43), kind=kOutput, calls=%fused_computation.1 | convolution fusion | flops 13631488 | bytes 4260096 | tf_op jit(solution)/shard_map/shde,shd->she/dot_general | solution.py:99
  94.6 0.1 subtract_multiply_fusion
  94.7 1.5 multiply_add_fusion
  96.2 0.0 copy-start.2
  96.2 0.0 copy-start.3
  96.2 2.0 copy-done.2
  98.2 3.6 %fusion.79 = f32[16,4,1,128]{3,2,1,0:T(1,128)S(1)} fusion(f32[16,4,128,128]{3,2,1,0:T(8,128)S(1)} %multiply_add_fusion, f32[16,4,128,1]{2,3,1,0:T(1,128)S(1)} %bitcast.86), kind=kOutput, calls=%fused_computation.121 | convolution fusion | flops 12582912 | bytes 4259840 | tf_op jit(solution)/shard_map/shde,shd->she/dot_general | solution.py:102
  101.8 0.1 multiply_reduce_fusion
  101.9 0.1 multiply_convert_fusion
  102.0 36.7 %all-gather.3.cloned.1.call-done = bf16[512,2048]{1,0:T(8,128)(2,1)} async-done(((bf16[512,256]{1,0:T(8,128)(2,1)}), bf16[512,2048]{1,0:T(8,128)(2,1)}) %all-gather.3.cloned.1.call-update) | async-done | bytes 2097168 | tf_op jit(solution)/shard_map/all_gather | solution.py:111
  138.7 2.0 convolution_convert_fusion.3
  140.7 5.8 %all-gather = bf16[64,2048]{1,0:T(8,128)(2,1)S(1)} all-gather(bf16[16,2048]{1,0:T(8,128)(2,1)S(1)} %convolution_convert_fusion.3), channel_id=2, replica_groups=mesh['ep'=8,'tp'=4] {'tp'}, dimensions={0}, use_global_device_ids=true | all-gather | bytes 327680 | tf_op jit(solution)/shard_map/all_gather | solution.py:117
  146.5 0.1 fusion.31
  146.7 0.1 fusion.33
  146.8 1.1 convolution_convert_fusion.1
  147.9 3.5 %all-to-all-start.1 = ((bf16[8,16,2048]{2,1,0:T(8,128)(2,1)}), bf16[8,16,2048]{2,1,0:T(8,128)(2,1)S(1)}, u32[]{:S(2)}, u32[]{:S(2)}) async-start(bf16[8,16,2048]{2,1,0:T(8,128)(2,1)} %bitcast.14), calls=%async_computation.2 | async-start | bytes 1048576 | tf_op jit(solution)/shard_map/all_to_all | solution.py:165
  151.4 0.0 copy-start.11
  151.4 0.0 copy-start.9
  151.4 0.0 all-reduce.3.cloned.1.call-start
  151.5 38.9 %all_gather.22 = bf16[2048,128]{1,0:T(8,128)(2,1)S(1)} all-gather(bf16[256,128]{1,0:T(8,128)(2,1)S(1)} %copy-done.6), channel_id=1, replica_groups=mesh['ep'=8,'tp'=4] {'ep'}, dimensions={0}, use_global_device_ids=true | all-gather | bytes 589824 | tf_op jit(solution)/shard_map/all_gather | solution.py:131
  190.4 31.4 %all_gather.23 = bf16[128,2048]{1,0:T(8,128)(2,1)S(1)} all-gather(bf16[128,256]{1,0:T(8,128)(2,1)S(1)} %copy-done.7), channel_id=1, replica_groups=mesh['ep'=8,'tp'=4] {'ep'}, dimensions={1}, use_global_device_ids=true | all-gather | bytes 589824 | tf_op jit(solution)/shard_map/all_gather | solution.py:137
  221.8 0.2 fusion.80
  222.0 1.0 convolution_convert_fusion.2
  222.9 0.0 all-to-all-done.1
  223.0 0.3 fusion.25
  223.3 2.4 convolution_convert_fusion
  225.6 0.0 all-reduce.3.cloned.1.call-update
  225.7 31.3 %all-reduce.3.cloned.1.call-done = (bf16[8,16,2048]{2,1,0:T(8,128)(2,1)}, bf16[16,2048]{1,0:T(8,128)(2,1)}) async-done(((bf16[8,16,2048]{2,1,0:T(8,128)(2,1)}, bf16[16,2048]{1,0:T(8,128)(2,1)}), (bf16[8,16,2048]{2,1,0:T(8,128)(2,1)}, bf16[16,2048]{1,0:T(8,128)(2,1)})) %all-reduce.3.cloned.1.call-update) | async-done | bytes 589840 | tf_op jit(solution)/shard_map/psum | solution.py:175
  257.0 5.5 %all-to-all-start.2 = ((bf16[8,16,2048]{2,1,0:T(8,128)(2,1)}), bf16[8,16,2048]{2,1,0:T(8,128)(2,1)S(1)}, u32[]{:S(2)}, u32[]{:S(2)}) async-start(bf16[8,16,2048]{2,1,0:T(8,128)(2,1)} %get-tuple-element.2), calls=%async_computation.3 | async-start | bytes 1048576 | tf_op jit(solution)/shard_map/all_to_all | solution.py:176
  262.6 0.1 fusion.13
  262.7 13.4 %all-to-all-done.2 = bf16[8,16,2048]{2,1,0:T(8,128)(2,1)S(1)} async-done(((bf16[8,16,2048]{2,1,0:T(8,128)(2,1)}), bf16[8,16,2048]{2,1,0:T(8,128)(2,1)S(1)}, u32[]{:S(2)}, u32[]{:S(2)}) %all-to-all-start.2) | async-done | bytes 524320 | tf_op jit(solution)/shard_map/all_to_all | solution.py:176
  276.1 0.3 fusion.3
  276.4 1.6 fusion.35
  (43 shorter events, 0.3 us)
Async XLA Ops:
  7.2 216.1 %copy-start = (bf16[1,128,2048]{2,1,0:T(8,128)(2,1)S(1)}, bf16[1,128,2048]{2,1,0:T(8,128)(2,1)}, u32[]{:S(2)}) copy-start(bf16[1,128,2048]{2,1,0:T(8,128)(2,1)} %param.41) | copy-start | bytes 1572868
  7.2 19.8 %copy-start.12 = (f32[4]{0:T(128)S(1)}, f32[4]{0:T(128)}, u32[]{:S(2)}) copy-start(f32[4]{0:T(128)} %param.31) | copy-start | bytes 52
  7.2 19.8 %copy-start.13 = (f32[4]{0:T(128)S(1)}, f32[4]{0:T(128)}, u32[]{:S(2)}) copy-start(f32[4]{0:T(128)} %param.32) | copy-start | bytes 52
  7.2 21.8 %copy-start.14 = (bf16[128]{0:T(256)(128)(2,1)S(1)}, bf16[128]{0:T(256)(128)(2,1)}, u32[]{:S(2)}) copy-start(bf16[128]{0:T(256)(128)(2,1)} %param.33) | copy-start | bytes 772
  7.2 21.8 %copy-start.10 = (bf16[2048]{0:T(1024)(128)(2,1)S(1)}, bf16[2048]{0:T(1024)(128)(2,1)}, u32[]{:S(2)}) copy-start(bf16[2048]{0:T(1024)(128)(2,1)} %param.36) | copy-start | bytes 12292
  7.2 21.9 %copy-start.8 = (s32[16,4]{0,1:T(4,128)S(1)}, s32[16,4]{0,1:T(4,128)}, u32[]{:S(2)}) copy-start(s32[16,4]{0,1:T(4,128)} %param.37) | copy-start | bytes 772
  7.2 22.5 %copy-start.5 = (bf16[256,128]{1,0:T(8,128)(2,1)S(1)}, bf16[256,128]{1,0:T(8,128)(2,1)}, u32[]{:S(2)}) copy-start(bf16[256,128]{1,0:T(8,128)(2,1)} %param.42) | copy-start | bytes 196612
  7.2 80.0 %reduce-scatter.2.cloned.1.call-start = ((), (), s32[]{:S(2)}) async-start(), calls=%async_computation.4 | async-start | bytes 884736 | tf_op jit(solution)/shard_map/reduce_scatter | solution.py:58
  26.3 112.5 %all-gather.3.cloned.1.call-start = ((), (), s32[]{:S(2)}) async-start(), calls=%async_computation.5 | async-start | bytes 2359296 | tf_op jit(solution)/shard_map/all_gather | solution.py:111
  88.3 6.3 %copy-start.1 = (f32[16,4,128,128]{3,2,1,0:T(8,128)S(1)}, f32[16,4,128,128]{3,2,1,0:T(8,128)}, u32[]{:S(2)}) copy-start(f32[16,4,128,128]{3,2,1,0:T(8,128)} %param.34) | copy-start | bytes 12582916
  96.2 2.0 copy-start.2
  96.2 50.3 %copy-start.3 = (bf16[16,2048]{1,0:T(8,128)(2,1)S(1)}, bf16[16,2048]{1,0:T(8,128)(2,1)}, u32[]{:S(2)}) copy-start(bf16[16,2048]{1,0:T(8,128)(2,1)} %param.23) | copy-start | bytes 196612
  98.2 53.3 %copy-start.6 = (bf16[256,128]{1,0:T(8,128)(2,1)S(1)}, bf16[256,128]{1,0:T(8,128)(2,1)}, u32[]{:S(2)}) copy-start(bf16[256,128]{1,0:T(8,128)(2,1)} %param.43) | copy-start | bytes 196612
  98.2 92.2 %copy-start.7 = (bf16[128,256]{1,0:T(8,128)(2,1)S(1)}, bf16[128,256]{1,0:T(8,128)(2,1)}, u32[]{:S(2)}) copy-start(bf16[128,256]{1,0:T(8,128)(2,1)} %param.44) | copy-start | bytes 196612
  101.8 121.1 %copy-start.4 = (bf16[1,2048,128]{2,1,0:T(8,128)(2,1)S(1)}, bf16[1,2048,128]{2,1,0:T(8,128)(2,1)}, u32[]{:S(2)}) copy-start(bf16[1,2048,128]{2,1,0:T(8,128)(2,1)} %param.39) | copy-start | bytes 1572868
  147.9 75.1 %all-to-all-start.1 = ((bf16[8,16,2048]{2,1,0:T(8,128)(2,1)}), bf16[8,16,2048]{2,1,0:T(8,128)(2,1)S(1)}, u32[]{:S(2)}, u32[]{:S(2)}) async-start(bf16[8,16,2048]{2,1,0:T(8,128)(2,1)} %bitcast.14), calls=%async_computation.2 | async-start | bytes 1048576 | tf_op jit(solution)/shard_map/all_to_all | solution.py:165
  151.4 111.2 %copy-start.11 = (bf16[2048]{0:T(1024)(128)(2,1)S(1)}, bf16[2048]{0:T(1024)(128)(2,1)}, u32[]{:S(2)}) copy-start(bf16[2048]{0:T(1024)(128)(2,1)} %param.45) | copy-start | bytes 12292
  151.4 111.2 %copy-start.9 = (f32[16,4]{0,1:T(4,128)S(1)}, f32[16,4]{0,1:T(4,128)}, u32[]{:S(2)}) copy-start(f32[16,4]{0,1:T(4,128)} %param.38) | copy-start | bytes 772
  151.4 105.6 %all-reduce.3.cloned.1.call-start = ((), (), s32[]{:S(2)}) async-start(), calls=%async_computation.6 | async-start | bytes 1179648 | tf_op jit(solution)/shard_map/psum | solution.py:175
  257.0 19.1 %all-to-all-start.2 = ((bf16[8,16,2048]{2,1,0:T(8,128)(2,1)}), bf16[8,16,2048]{2,1,0:T(8,128)(2,1)S(1)}, u32[]{:S(2)}, u32[]{:S(2)}) async-start(bf16[8,16,2048]{2,1,0:T(8,128)(2,1)} %get-tuple-element.2), calls=%async_computation.3 | async-start | bytes 1048576 | tf_op jit(solution)/shard_map/all_to_all | solution.py:176
Sparse Core Ops, SparseCore 0:
  26.4 60.8 reduce-scatter.1
  89.3 49.3 all-gather.2
  225.8 31.1 all-reduce.2
